TPU v7x, 32 devices: a whole 2x2x4 slice. The times are simulated.
32 devices in a mesh: ep: 8 (over z, x), tp: 4 (over y, core).
Axes of the slice: x: 2, y: 2, z: 4, core: 2. Of those that a mesh axis runs over, the one named last changes fastest.
Arguments:
- tokens: bfloat16 [128, 2048], P('ep'), may hold values from -6 to 6
- norm1_gain: float32 [2048], replicated, may hold values from 0.1 to 1.9
- query_weight: bfloat16 [2048, 512], P(None, 'tp'), may hold values from -0.125 to 0.125
- key_weight: bfloat16 [2048, 256], P(None, 'tp'), may hold values from -0.125 to 0.125
- value_weight: bfloat16 [2048, 256], P(None, 'tp'), may hold values from -0.125 to 0.125
- forget_weight: bfloat16 [2048, 8], P(None, 'tp'), may hold values from -0.125 to 0.125
- forget_bias: float32 [8], P('tp'), may hold values from 0.5 to 4
- out_weight: bfloat16 [512, 2048], P('tp'), may hold values from -0.25 to 0.25
- kv_cache: bfloat16 [128, 1024, 4, 128], P('ep', None, 'tp'), may hold values from -6 to 6
- log_gates: float32 [128, 8, 1024], P('ep', 'tp'), may hold values from -1024 to 0, as said below
- lengths: int32 [128], P('ep'), may hold values from 64 to 1024
- norm2_gain: float32 [2048], replicated, may hold values from 0.1 to 1.9
- routing: int32 [128, 4], P('ep'), may hold values from 0 to 7, all different within a row; in each aligned block of 16 rows (0 to 15, 16 to 31, ...) at most 16 rows name the same one
- route_weight: float32 [128, 4], P('ep'), may hold values from 0.1 to 0.6
- expert_gate: bfloat16 [8, 2048, 2048], P('ep', None, 'tp'), may hold values from -0.25 to 0.25
- expert_up: bfloat16 [8, 2048, 2048], P('ep', None, 'tp'), may hold values from -0.25 to 0.25
- expert_down: bfloat16 [8, 2048, 2048], P('ep', 'tp'), may hold values from -0.0625 to 0.0625
- dense_gate: bfloat16 [2048, 4096], P(None, 'ep'), may hold values from -0.25 to 0.25
- dense_up: bfloat16 [2048, 4096], P(None, 'ep'), may hold values from -0.25 to 0.25
- dense_down: bfloat16 [4096, 2048], P('ep'), may hold values from -0.09375 to 0.09375
- dense_mix: float32 [2048], replicated, may hold values from -0.125 to 0.125
Outputs:
- layer_out: bfloat16 [128, 2048], P(('ep', 'tp'))
Inputs may be any that keep to these rules, and one draw needn't show every extreme that they name: `log_gates`: Non-increasing along the positions. `routing`: each row names 4 different experts. Among the rows of one index of ep (aligned blocks of 16 rows) no expert is named by more than 16 rows, and in every draw some expert is named by exactly 16 rows of some block.
All inputs are finite; a program needn't handle non-finite values.
Results may differ from a plain program's by a relative error of at most 0.011.
Values may be sent and summed in bfloat16 or wider, within the bound.
No kernel may reach another device: no remote copies, remote signals or barrier semaphores. Data moves between devices by JAX's collectives and lax.ppermute only.
A program may use at most 128 MiB of HBM per device.

v0:
```python
import jax
import jax.numpy as jnp
from jax import lax
from jax.sharding import PartitionSpec as P

EPS = 1e-05
LIMIT = 7.0
ALPHA = 1.702


def clamped_unit(gate_pre, up_pre):
    capped = jnp.minimum(gate_pre, LIMIT)
    return capped * jax.nn.sigmoid(ALPHA * capped) * (jnp.clip(up_pre, -LIMIT, LIMIT) + 1.0)


def rms_scaled(values, gain_vec):
    return values * lax.rsqrt(jnp.mean(values * values, axis=-1, keepdims=True) + EPS) * gain_vec


def slot_tables(routes, experts, capacity):
    flat_ids = routes.reshape(-1)
    onehot = (flat_ids[:, None] == jnp.arange(experts, dtype=jnp.int32)[None, :]).astype(jnp.int32)
    earlier = jnp.cumsum(onehot, axis=0, dtype=jnp.int32) - onehot
    slot_ids = jnp.sum(earlier * onehot, axis=1, dtype=jnp.int32)
    matches = onehot[:, :, None] * (
        slot_ids[:, None, None] == jnp.arange(capacity, dtype=jnp.int32)[None, None, :]
    ).astype(jnp.int32)
    owners = jnp.arange(flat_ids.shape[0], dtype=jnp.int32) // routes.shape[1]
    source = jnp.sum(matches * owners[:, None, None], axis=0, dtype=jnp.int32)
    return (slot_ids, source)


def on_device(
    tokens,
    norm1_gain,
    query_weight,
    key_weight,
    value_weight,
    forget_weight,
    forget_bias,
    out_weight,
    kv_cache,
    log_gates,
    lengths,
    norm2_gain,
    routing,
    route_weight,
    expert_gate,
    expert_up,
    expert_down,
    dense_gate,
    dense_up,
    dense_down,
    dense_mix,
):
    seq_count, model_width = tokens.shape
    tp_count = lax.axis_size("tp")
    ep_count = lax.axis_size("ep")
    own_rows = seq_count // tp_count
    row_start = lax.axis_index("tp") * own_rows
    local_heads = forget_bias.shape[0]
    kv_local = kv_cache.shape[2]
    head_dim = kv_cache.shape[3] // 2
    per_kv = local_heads // kv_local
    cache_len = kv_cache.shape[1]
    score_scale = head_dim ** (-0.5)
    normed = rms_scaled(tokens.astype(jnp.float32), norm1_gain).astype(jnp.bfloat16)
    queries = jnp.dot(normed, query_weight, preferred_element_type=jnp.float32).astype(jnp.bfloat16)
    queries = queries.reshape(seq_count, kv_local, per_kv, head_dim)
    key_new = jnp.dot(normed, key_weight, preferred_element_type=jnp.float32).astype(jnp.bfloat16)
    key_new = key_new.reshape(seq_count, kv_local, head_dim)
    value_new = jnp.dot(normed, value_weight, preferred_element_type=jnp.float32).astype(
        jnp.bfloat16
    )
    value_new = value_new.reshape(seq_count, kv_local, head_dim)
    gate_new = jax.nn.log_sigmoid(
        jnp.dot(normed, forget_weight, preferred_element_type=jnp.float32) + forget_bias
    )
    scores = (
        jnp.einsum(
            "skgd,slkd->skgl", queries, kv_cache[..., :head_dim], preferred_element_type=jnp.float32
        )
        * score_scale
    )
    last_index = jnp.broadcast_to((lengths - 1)[:, None, None], (seq_count, local_heads, 1))
    last_gate = jnp.take_along_axis(log_gates, last_index, axis=2)
    gate_bias = (last_gate - log_gates + gate_new[:, :, None]).reshape(
        seq_count, kv_local, per_kv, cache_len
    )
    live_mask = (jnp.arange(cache_len, dtype=jnp.int32)[None, :] < lengths[:, None])[
        :, None, None, :
    ]
    cached = jnp.where(live_mask, jnp.exp(scores + gate_bias), 0.0)
    own_exp = jnp.exp(
        jnp.einsum("skgd,skd->skg", queries, key_new, preferred_element_type=jnp.float32)
        * score_scale
    )
    denominator = jnp.sum(cached, axis=-1) + own_exp
    weight_cache = (cached / denominator[..., None]).astype(jnp.bfloat16)
    weight_own = (own_exp / denominator).astype(jnp.bfloat16)
    attended = jnp.einsum(
        "skgl,slkd->skgd",
        weight_cache,
        kv_cache[..., head_dim:],
        preferred_element_type=jnp.float32,
    )
    attended = (
        attended
        + weight_own.astype(jnp.float32)[..., None] * value_new.astype(jnp.float32)[:, :, None, :]
    )
    attended = attended.astype(jnp.bfloat16).reshape(seq_count, local_heads * head_dim)
    partial_out = jnp.dot(attended, out_weight, preferred_element_type=jnp.float32)
    attn_out = lax.psum(partial_out, "tp").astype(jnp.bfloat16)
    residual = tokens.astype(jnp.float32) + attn_out.astype(jnp.float32)
    hidden_in = rms_scaled(residual, norm2_gain).astype(jnp.bfloat16)
    own_hidden = lax.dynamic_slice_in_dim(hidden_in, row_start, own_rows, 0)
    own_residual = lax.dynamic_slice_in_dim(residual, row_start, own_rows, 0)
    row_piece = lax.all_gather(own_hidden, "ep", axis=0, tiled=True)
    gate_pre = jnp.dot(row_piece, dense_gate, preferred_element_type=jnp.float32)
    up_pre = jnp.dot(row_piece, dense_up, preferred_element_type=jnp.float32)
    dense_act = clamped_unit(gate_pre, up_pre).astype(jnp.bfloat16)
    dense_val = lax.psum_scatter(
        jnp.dot(dense_act, dense_down, preferred_element_type=jnp.float32),
        "ep",
        scatter_dimension=0,
        tiled=True,
    )
    local_experts = expert_gate.shape[0]
    experts = local_experts * ep_count
    top_count = routing.shape[1]
    capacity = min(seq_count, seq_count * top_count * 3 // experts)
    slot_ids, source = slot_tables(routing, experts, capacity)
    dispatch = hidden_in[source.reshape(-1)].reshape(experts, capacity, model_width)
    received = lax.all_to_all(dispatch, "ep", split_axis=0, concat_axis=0, tiled=True)
    item_count = received.shape[1]
    grouped = received.reshape(ep_count, local_experts, item_count, model_width)
    gate_pre = jnp.einsum(
        "sjnd,jdf->sjnf", grouped, expert_gate, preferred_element_type=jnp.float32
    )
    up_pre = jnp.einsum("sjnd,jdf->sjnf", grouped, expert_up, preferred_element_type=jnp.float32)
    activation = clamped_unit(gate_pre, up_pre).astype(jnp.bfloat16)
    partial_units = jnp.einsum(
        "sjnf,jfd->sjnd", activation, expert_down, preferred_element_type=jnp.float32
    )
    partial_units = partial_units.reshape(ep_count * local_experts, item_count, model_width)
    slot_index = routing * capacity + slot_ids.reshape(seq_count, top_count)
    shares = lax.psum_scatter(
        partial_units.astype(jnp.bfloat16), "tp", scatter_dimension=2, tiled=True
    )
    returned = lax.all_to_all(shares, "ep", split_axis=0, concat_axis=0, tiled=True)
    share_width = returned.shape[2]
    picked = returned.reshape(experts * capacity, share_width)[slot_index.reshape(-1)]
    picked = picked.reshape(seq_count, top_count, share_width)
    moe_cols = jnp.sum(route_weight[..., None] * picked.astype(jnp.float32), axis=1)
    moe_val = lax.all_to_all(
        moe_cols.astype(jnp.bfloat16), "tp", split_axis=0, concat_axis=1, tiled=True
    ).astype(moe_cols.dtype)
    mix_gate = jax.nn.sigmoid(
        jnp.dot(own_hidden.astype(jnp.float32), dense_mix, precision=lax.Precision.HIGHEST)
    )
    return (own_residual + moe_val + mix_gate[:, None] * dense_val).astype(jnp.bfloat16)


def solution(mesh):
    return jax.shard_map(
        on_device,
        mesh=mesh,
        in_specs=(
            P("ep", None),
            P(),
            P(None, "tp"),
            P(None, "tp"),
            P(None, "tp"),
            P(None, "tp"),
            P("tp"),
            P("tp", None),
            P("ep", None, "tp", None),
            P("ep", "tp", None),
            P("ep"),
            P(),
            P("ep", None),
            P("ep", None),
            P("ep", None, "tp"),
            P("ep", None, "tp"),
            P("ep", "tp", None),
            P(None, "ep"),
            P(None, "ep"),
            P("ep", None),
            P(),
        ),
        out_specs=P(("ep", "tp"), None),
        check_vma=False,
    )
```

profile of v0, /device:TPU:0, one launch (start us, length us, event | category | flops | bytes accessed | tf_op | source)
XLA Modules:
  0.0 175.3 jit_solution(10059559181539150195)
XLA Ops:
  7.4 0.8 broadcast_add_fusion
  8.2 0.7 broadcast_compare_fusion
  8.8 0.7 iota_compare_fusion
  9.6 0.1 copy.44
  9.7 0.1 reshape.457
  9.8 0.0 copy-start.4
  9.8 0.0 copy-start.5
  9.9 0.0 copy-start.10
  9.9 0.0 copy-start.11
  9.9 1.8 %gather_fusion.2 = f32[32]{0:T(128)S(1)} fusion(f32[16,2,1024]{2,1,0:T(2,128)} %param.30, s32[32]{0:T(128)S(1)} %reshape.457), kind=kCustom, calls=%fused_computation.2 | custom fusion | bytes 640 | tf_op jit(solution)/shard_map/jit(take_along_axis)/gather | solution.py:86
  11.7 0.1 gather.13
  11.8 0.1 fusion.97
  11.9 0.0 copy-done.2
  11.9 0.1 fusion.72
  12.1 0.2 convolution_convert_fusion.3
  12.3 0.1 reshape.424
  12.4 0.2 fusion.102
  12.6 0.1 copy.45
  12.7 0.2 fusion.55
  12.9 0.2 fusion.54
  13.2 0.1 fusion.98
  13.3 3.6 %fusion.123 = (f32[16,2]{1,0:T(8,128)S(1)}, f32[16,2,1024]{2,1,0:T(2,128)S(1)}) fusion(f32[16,2]{1,0:T(8,128)S(1)} %copy.45, f32[16,2,1024]{2,1,0:T(2,128)S(1)} %copy-done.1, f32[16,2]{1,0:T(8,128)S(1)} %fusion.97, bf16[16,2,64]{2,1,0:T(2,128)(2,1)S(1)} %reshape.424, bf16[16,1024,1,128]{3,1,2,0:T(8,128)(2,1)} %param.29, ...), kind=kOutput, calls=%fused_computation.138 | convolution fusion | flops 4390880 | bytes 4477312 | tf_op jit(solution)/shard_map/skgd,slkd->skgl/dot_general | solution.py:80
  17.0 0.0 copy-start.7
  17.0 1.4 fusion.51
  18.4 0.1 reshape.427
  18.5 0.2 fusion.124
  18.7 14.5 %all-reduce.5 = bf16[16,2048]{1,0:T(8,128)(2,1)S(1)} all-reduce(f32[16,2048]{1,0:T(8,128)S(1)} %fusion.124), channel_id=1, replica_groups=mesh['ep'=8,'tp'=4] {'tp'}, use_global_device_ids=true, to_apply=%region_2.3 | all-reduce | flops 32768 | bytes 196608 | tf_op jit(solution)/shard_map/psum | solution.py:113
  33.2 0.1 multiply_reduce_fusion.1
  33.3 0.1 copy.48
  33.4 0.1 eq.37
  33.5 0.1 fusion.93
  33.6 0.1 copy.49
  33.7 0.1 reduce_window_sum.11
  33.8 0.2 select_reduce_fusion
  34.0 0.2 multiply_reduce_fusion.2
  34.2 0.1 reshape.428
  34.3 0.1 multiply_convert_fusion
  34.4 0.9 gather_fusion
  35.3 19.1 %all_to_all.20 = bf16[8,16,2048]{2,1,0:T(8,128)(2,1)S(1)} all-to-all(bf16[8,16,2048]{2,1,0:T(8,128)(2,1)S(1)} %bitcast.124), channel_id=1, replica_groups=mesh['ep'=8,'tp'=4] {'ep'}, dimensions={0} | all-to-all | bytes 1048576 | tf_op jit(solution)/shard_map/all_to_all | solution.py:134
  54.4 2.0 %fusion.14 = f32[8,1,16,512]{3,2,0,1:T(8,128)S(1)} fusion(bf16[8,16,2048]{2,1,0:T(8,128)(2,1)S(1)} %all_to_all.20, bf16[1,2048,512]{2,1,0:T(8,128)(2,1)} %param.35), kind=kOutput, calls=%fused_computation.16 | convolution fusion | flops 268500992 | bytes 2883584 | tf_op jit(solution)/shard_map/sjnd,jdf->sjnf/dot_general | solution.py:137
  56.4 3.2 %convolution_convert_fusion = bf16[8,16,2048]{2,1,0:T(8,128)(2,1)} fusion(bf16[1,512,2048]{2,1,0:T(8,128)(2,1)S(1)} %copy-done, bf16[8,16,2048]{2,1,0:T(8,128)(2,1)S(1)} %all_to_all.20, bf16[1,2048,512]{2,1,0:T(8,128)(2,1)} %param.36, f32[8,1,16,512]{3,2,0,1:T(8,128)S(1)} %fusion.14), kind=kOutput, calls=%fused_computation.9 | convolution fusion | flops 537722880 | bytes 5505024 | tf_op jit(solution)/shard_map/sjnf,jfd->sjnd/dot_general | solution.py:142
  59.6 0.0 reduce-scatter.2.cloned.1.call-update
  59.7 0.0 all-reduce.4.cloned.1.call-start
  59.8 30.5 %all-gather = bf16[8,4,2048]{2,1,0:T(4,128)(2,1)S(1)} all-gather(bf16[1,4,2048]{2,1,0:T(4,128)(2,1)S(1)} %dynamic-slice_bitcast_fusion), channel_id=1, replica_groups=mesh['ep'=8,'tp'=4] {'ep'}, dimensions={0}, use_global_device_ids=true | all-gather | bytes 147456 | tf_op jit(solution)/shard_map/all_gather | solution.py:118
  90.3 2.0 %convolution_minimum_fusion = f32[32,512]{1,0:T(8,128)S(1)} fusion(bf16[32,2048]{1,0:T(8,128)(2,1)S(1)} %reshape.466, bf16[2048,512]{1,0:T(8,128)(2,1)} %param.38), kind=kOutput, calls=%fused_computation.29 | convolution fusion | flops 67125248 | bytes 2293760 | tf_op jit(solution)/shard_map/dot_general | solution.py:119
  92.4 0.0 copy-start.8
  92.4 0.0 copy-start.15
  92.4 3.9 %fusion.47 = f32[32,2048]{1,0:T(8,128)} fusion(bf16[512,2048]{1,0:T(8,128)(2,1)} %param.40, bf16[32,2048]{1,0:T(8,128)(2,1)S(1)} %reshape.466, bf16[2048,512]{1,0:T(8,128)(2,1)} %param.39, f32[32,512]{1,0:T(8,128)S(1)} %convolution_minimum_fusion), kind=kOutput, calls=%fused_computation.31 | convolution fusion | flops 134365184 | bytes 4653056 | tf_op jit(solution)/shard_map/dot_general | solution.py:123
  96.3 0.0 all-reduce.4.cloned.1.call-update
  96.3 0.1 reshape.435
  96.4 0.1 reshape.436
  96.5 0.1 copy.47
  96.6 3.6 %all-to-all-start.1 = ((bf16[8,16,512]{2,1,0:T(8,128)(2,1)}), bf16[8,16,512]{2,1,0:T(8,128)(2,1)S(1)}, u32[]{:S(2)}, u32[]{:S(2)}) async-start(bf16[8,16,512]{2,1,0:T(8,128)(2,1)} %reduce-scatter.2.cloned.1.call-done), calls=%async_computation.2 | async-start | bytes 262144 | tf_op jit(solution)/shard_map/all_to_all | solution.py:150
  100.2 7.5 %all-to-all-done.1 = bf16[8,16,512]{2,1,0:T(8,128)(2,1)S(1)} async-done(((bf16[8,16,512]{2,1,0:T(8,128)(2,1)}), bf16[8,16,512]{2,1,0:T(8,128)(2,1)S(1)}, u32[]{:S(2)}, u32[]{:S(2)}) %all-to-all-start.1) | async-done | bytes 131104 | tf_op jit(solution)/shard_map/all_to_all | solution.py:150
  107.7 0.7 gather_fusion.1
  108.5 0.2 multiply_reduce_fusion
  108.6 0.6 convert_element_type.115
  109.2 3.3 %all-to-all-start.2 = ((bf16[4,4,512]{2,1,0:T(4,128)(2,1)}), bf16[4,4,512]{2,1,0:T(4,128)(2,1)S(1)}, u32[]{:S(2)}, u32[]{:S(2)}) async-start(bf16[4,4,512]{2,1,0:T(4,128)(2,1)} %convert_element_type.115), calls=%async_computation.3 | async-start | bytes 32768 | tf_op jit(solution)/shard_map/all_to_all | solution.py:155
  112.5 0.1 fusion.60
  112.6 0.1 copy-done.15
  112.7 0.6 dynamic-slice
  113.9 2.5 %all-to-all-done.2 = bf16[4,4,512]{2,1,0:T(4,128)(2,1)S(1)} async-done(((bf16[4,4,512]{2,1,0:T(4,128)(2,1)}), bf16[4,4,512]{2,1,0:T(4,128)(2,1)S(1)}, u32[]{:S(2)}, u32[]{:S(2)}) %all-to-all-start.2) | async-done | bytes 16416 | tf_op jit(solution)/shard_map/all_to_all | solution.py:155
  116.3 50.0 %all-reduce.4.cloned.1.call-done = f32[32,2048]{1,0:T(8,128)} async-done(((f32[32,2048]{1,0:T(8,128)}), f32[32,2048]{1,0:T(8,128)}) %all-reduce.4.cloned.1.call-update) | async-done | bytes 262160
  166.4 1.5 fusion.88
  (44 shorter events, 0.3 us)
Async XLA Ops:
  7.4 49.1 %copy-start = (bf16[1,512,2048]{2,1,0:T(8,128)(2,1)S(1)}, bf16[1,512,2048]{2,1,0:T(8,128)(2,1)}, u32[]{:S(2)}) copy-start(bf16[1,512,2048]{2,1,0:T(8,128)(2,1)} %param.37) | copy-start | bytes 6291460
  7.4 89.2 %reduce-scatter.2.cloned.1.call-start = ((), (), s32[]{:S(2)}) async-start(), calls=%async_computation.4 | async-start | bytes 655360 | tf_op jit(solution)/shard_map/reduce_scatter | solution.py:147
  9.8 2.1 %copy-start.2 = (bf16[16,2048]{1,0:T(8,128)(2,1)S(1)}, bf16[16,2048]{1,0:T(8,128)(2,1)}, u32[]{:S(2)}) copy-start(bf16[16,2048]{1,0:T(8,128)(2,1)} %param.21) | copy-start | bytes 196612
  9.8 2.2 %copy-start.4 = (bf16[2048,128]{1,0:T(8,128)(2,1)S(1)}, bf16[2048,128]{1,0:T(8,128)(2,1)}, u32[]{:S(2)}) copy-start(bf16[2048,128]{1,0:T(8,128)(2,1)} %param.23) | copy-start | bytes 1572868
  9.8 2.2 %copy-start.5 = (f32[2048]{0:T(1024)S(1)}, f32[2048]{0:T(1024)}, u32[]{:S(2)}) copy-start(f32[2048]{0:T(1024)} %param.22) | copy-start | bytes 24580
  9.9 2.5 %copy-start.12 = (bf16[2048,2]{0,1:T(2,128)(2,1)S(1)}, bf16[2048,2]{0,1:T(2,128)(2,1)}, u32[]{:S(2)}) copy-start(bf16[2048,2]{0,1:T(2,128)(2,1)} %param.26) | copy-start | bytes 24580
  9.9 2.5 %copy-start.14 = (f32[2]{0:T(128)S(1)}, f32[2]{0:T(128)}, u32[]{:S(2)}) copy-start(f32[2]{0:T(128)} %param.27) | copy-start | bytes 28
  9.9 2.8 %copy-start.10 = (bf16[2048,64]{0,1:T(8,128)(2,1)S(1)}, bf16[2048,64]{0,1:T(8,128)(2,1)}, u32[]{:S(2)}) copy-start(bf16[2048,64]{0,1:T(8,128)(2,1)} %param.24) | copy-start | bytes 786436
  9.9 3.0 %copy-start.11 = (bf16[2048,64]{0,1:T(8,128)(2,1)S(1)}, bf16[2048,64]{0,1:T(8,128)(2,1)}, u32[]{:S(2)}) copy-start(bf16[2048,64]{0,1:T(8,128)(2,1)} %param.25) | copy-start | bytes 786436
  9.9 3.4 %copy-start.1 = (f32[16,2,1024]{2,1,0:T(2,128)S(1)}, f32[16,2,1024]{2,1,0:T(2,128)}, u32[]{:S(2)}) copy-start(f32[16,2,1024]{2,1,0:T(2,128)} %param.30) | copy-start | bytes 393220
  13.3 3.7 %copy-start.9 = (bf16[16,1024,1,128]{3,1,2,0:T(8,128)(2,1)S(1)}, bf16[16,1024,1,128]{3,1,2,0:T(8,128)(2,1)}, u32[]{:S(2)}) copy-start(bf16[16,1024,1,128]{3,1,2,0:T(8,128)(2,1)} %param.29) | copy-start | bytes 12582916
  17.0 1.5 copy-start.3
  17.0 16.3 %copy-start.7 = (s32[16,4]{0,1:T(4,128)S(1)}, s32[16,4]{0,1:T(4,128)}, u32[]{:S(2)}) copy-start(s32[16,4]{0,1:T(4,128)} %param.33) | copy-start | bytes 772
  17.0 17.3 %copy-start.6 = (f32[2048]{0:T(1024)S(1)}, f32[2048]{0:T(1024)}, u32[]{:S(2)}) copy-start(f32[2048]{0:T(1024)} %param.32) | copy-start | bytes 24580
  59.7 106.7 %all-reduce.4.cloned.1.call-start = ((), (), s32[]{:S(2)}) async-start(), calls=%async_computation.5 | async-start | bytes 524288
  92.4 4.1 %copy-start.8 = (f32[16,4]{0,1:T(4,128)S(1)}, f32[16,4]{0,1:T(4,128)}, u32[]{:S(2)}) copy-start(f32[16,4]{0,1:T(4,128)} %param.34) | copy-start | bytes 772
  92.4 20.1 %copy-start.13 = (f32[2048]{0:T(1024)S(1)}, f32[2048]{0:T(1024)}, u32[]{:S(2)}) copy-start(f32[2048]{0:T(1024)} %param.41) | copy-start | bytes 24580
  92.4 20.3 %copy-start.15 = (u32[32]{0:T(128)S(1)}, u32[32]{0:T(128)}, u32[]{:S(2)}) copy-start(u32[32]{0:T(128)} %constant.108) | copy-start | bytes 388
  96.6 11.1 %all-to-all-start.1 = ((bf16[8,16,512]{2,1,0:T(8,128)(2,1)}), bf16[8,16,512]{2,1,0:T(8,128)(2,1)S(1)}, u32[]{:S(2)}, u32[]{:S(2)}) async-start(bf16[8,16,512]{2,1,0:T(8,128)(2,1)} %reduce-scatter.2.cloned.1.call-done), calls=%async_computation.2 | async-start | bytes 262144 | tf_op jit(solution)/shard_map/all_to_all | solution.py:150
  109.2 7.1 %all-to-all-start.2 = ((bf16[4,4,512]{2,1,0:T(4,128)(2,1)}), bf16[4,4,512]{2,1,0:T(4,128)(2,1)S(1)}, u32[]{:S(2)}, u32[]{:S(2)}) async-start(bf16[4,4,512]{2,1,0:T(4,128)(2,1)} %convert_element_type.115), calls=%async_computation.3 | async-start | bytes 32768 | tf_op jit(solution)/shard_map/all_to_all | solution.py:155
Sparse Core Ops, SparseCore 0:
  59.8 20.9 reduce-scatter.1
Sparse Core Ops, SparseCore 1:
  96.4 69.9 all-reduce.3
where the time goes:
time: 176 us; the launch traced here: 175 us
  blocking collectives  64.1 us (36%)
  waiting for transfers between devices  60 us (34%)
  matrix products  17.5 us (10%)
  between operations  15.8 us (9%)
  starting transfers between devices  6.94 us (4%)
  local copies, waits for them, and re-layouts  6 us (3%)
  other arithmetic  4.98 us (3%)
    unnamed x3, waiting for transfers between devices  50.1 us
    all_gather x1, blocking collectives, on_device(): row_piece = lax.all_gather(own_hidden, 'ep', axis=0, tiled=True)  30.5 us
    all_to_all x1, blocking collectives, on_device(): lax.all_to_all(dispatch, 'ep', split_axis=0, concat_axis=0, tiled=True)  19.1 us
    psum x1, blocking collectives, on_device(): attn_out = lax.psum(partial_out, 'tp').astype(jnp.bfloat16)  14.5 us
    all_to_all x1, waiting for transfers between devices, on_device(): lax.all_to_all(shares, 'ep', split_axis=0, concat_axis=0, tiled=True)  7.48 us
    dot_general x1, matrix products, on_device(): jnp.dot(dense_act, dense_down, preferred_element_type=jnp.float32)  3.85 us
    all_to_all x1, starting transfers between devices, on_device(): lax.all_to_all(shares, 'ep', split_axis=0, concat_axis=0, tiled=True)  3.64 us
    dot_general x1, matrix products, on_device(): jnp.einsum('skgd,slkd->skgl', queries, kv_cache[..., :head_dim], preferre...  3.63 us
  transfers between devices with their start and end apart: 4, of which 3 were waited for; matrix products, arithmetic and copies ran while one was open for 5% of the time, Pallas kernels for 0%

commit v1 on v0

--- a/solution.py
+++ b/solution.py
@@ -115,7 +115,8 @@
     hidden_in = rms_scaled(residual, norm2_gain).astype(jnp.bfloat16)
     own_hidden = lax.dynamic_slice_in_dim(hidden_in, row_start, own_rows, 0)
     own_residual = lax.dynamic_slice_in_dim(residual, row_start, own_rows, 0)
-    row_piece = lax.all_gather(own_hidden, "ep", axis=0, tiled=True)
+    stack = jnp.stack([own_hidden] * lax.axis_size("ep"))
+    row_piece = jnp.concatenate(lax.all_to_all(stack, "ep", 0, 0), axis=0)
     gate_pre = jnp.dot(row_piece, dense_gate, preferred_element_type=jnp.float32)
     up_pre = jnp.dot(row_piece, dense_up, preferred_element_type=jnp.float32)
     dense_act = clamped_unit(gate_pre, up_pre).astype(jnp.bfloat16)

time: 176 us -> 172 us (0.977)
  blocking collectives: 64.1 us -> 14.5 us
  waiting for transfers between devices: 60 us -> 92.7 us
  starting transfers between devices: 6.94 us -> 18.3 us
    all_gather x1 -> x0, blocking collectives: 30.5 us -> none  [on_device(): row_piece = lax.all_gather(own_hidden, 'ep', axis=0, tiled=True)]
    all_to_all x0 -> x2, waiting for transfers between devices: none -> 20.4 us  [the longest x1 13.4 us: on_device(): lax.all_to_all(dispatch, 'ep', split_axis=0, concat_axis=0, tiled=True)]
    all_to_all x1 -> x0, blocking collectives: 19.1 us -> none  [on_device(): lax.all_to_all(dispatch, 'ep', split_axis=0, concat_axis=0, tiled=True)]
    all_to_all x0 -> x2, starting transfers between devices: none -> 9.49 us  [the longest x1 5.81 us: on_device(): lax.all_to_all(dispatch, 'ep', split_axis=0, concat_axis=0, tiled=True)]
    unnamed x3, waiting for transfers between devices: 50.1 us -> 59.2 us
    reduce_scatter x1, waiting for transfers between devices: 0.01 us -> 7.28 us  [on_device(): lax.psum_scatter(partial_units.astype(jnp.bfloat16), 'tp', scatter_dimens...]
    all_to_all x1, waiting for transfers between devices: 7.48 us -> 3.42 us  [on_device(): lax.all_to_all(shares, 'ep', split_axis=0, concat_axis=0, tiled=True)]
    all_to_all x1, starting transfers between devices: 3.64 us -> 5.51 us  [on_device(): lax.all_to_all(shares, 'ep', split_axis=0, concat_axis=0, tiled=True)]
  transfers between devices with their start and end apart: 4 -> 6, of which waited for: 3 -> 6; matrix products, arithmetic and copies ran while one was open for 5% -> 5% of each run, Pallas kernels for 0% -> 0%
where the time goes in v1:
time: 172 us; the launch traced here: 171 us
  waiting for transfers between devices  92.7 us (54%)
  starting transfers between devices  18.3 us (11%)
  matrix products  17.5 us (10%)
  between operations  15.9 us (9%)
  blocking collectives  14.5 us (8%)
  local copies, waits for them, and re-layouts  7.54 us (4%)
  other arithmetic  4.98 us (3%)
    unnamed x3, waiting for transfers between devices  59.2 us
    psum x1, blocking collectives, on_device(): attn_out = lax.psum(partial_out, 'tp').astype(jnp.bfloat16)  14.5 us
    all_to_all x1, waiting for transfers between devices, on_device(): lax.all_to_all(dispatch, 'ep', split_axis=0, concat_axis=0, tiled=True)  13.4 us
    reduce_scatter x1, waiting for transfers between devices, on_device(): lax.psum_scatter(partial_units.astype(jnp.bfloat16), 'tp', scatter_dimens...  7.28 us
    all_to_all x1, waiting for transfers between devices, on_device(): row_piece = jnp.concatenate(lax.all_to_all(stack, 'ep', 0, 0), axis=0)  7.05 us
    all_to_all x1, starting transfers between devices, on_device(): lax.all_to_all(dispatch, 'ep', split_axis=0, concat_axis=0, tiled=True)  5.81 us
    all_to_all x1, starting transfers between devices, on_device(): lax.all_to_all(shares, 'ep', split_axis=0, concat_axis=0, tiled=True)  5.51 us
    dot_general x1, matrix products, on_device(): jnp.dot(dense_act, dense_down, preferred_element_type=jnp.float32)  3.83 us
  transfers between devices with their start and end apart: 6, of which 6 were waited for; matrix products, arithmetic and copies ran while one was open for 5% of the time, Pallas kernels for 0%

profile of v1, /device:TPU:0, one launch (start us, length us, event | category | flops | bytes accessed | tf_op | source)
XLA Modules:
  0.0 171.4 jit_solution(1168365458000044869)
XLA Ops:
  7.4 0.8 broadcast_add_fusion
  8.2 0.7 broadcast_compare_fusion
  8.8 0.7 iota_compare_fusion
  9.6 0.1 copy.44
  9.7 0.1 reshape.463
  9.8 0.0 copy-start.2
  9.9 1.8 %gather_fusion.2 = f32[32]{0:T(128)S(1)} fusion(f32[16,2,1024]{2,1,0:T(2,128)} %param.30, s32[32]{0:T(128)S(1)} %reshape.463), kind=kCustom, calls=%fused_computation.2 | custom fusion | bytes 640 | tf_op jit(solution)/shard_map/jit(take_along_axis)/gather | solution.py:86
  11.7 0.1 gather.13
  11.8 0.1 fusion.96
  11.9 0.0 copy-done.2
  11.9 0.1 fusion.72
  12.1 0.2 convolution_convert_fusion.3
  12.3 0.1 reshape.429
  12.4 0.2 fusion.101
  12.6 0.1 copy.45
  12.7 0.2 fusion.55
  12.9 0.2 fusion.54
  13.2 0.1 fusion.97
  13.3 3.6 %fusion.121 = (f32[16,2]{1,0:T(8,128)S(1)}, f32[16,2,1024]{2,1,0:T(2,128)S(1)}) fusion(f32[16,2]{1,0:T(8,128)S(1)} %copy.45, f32[16,2,1024]{2,1,0:T(2,128)S(1)} %copy-done.1, f32[16,2]{1,0:T(8,128)S(1)} %fusion.96, bf16[16,2,64]{2,1,0:T(2,128)(2,1)S(1)} %reshape.429, bf16[16,1024,1,128]{3,1,2,0:T(8,128)(2,1)} %param.29, ...), kind=kOutput, calls=%fused_computation.136 | convolution fusion | flops 4390880 | bytes 4477312 | tf_op jit(solution)/shard_map/skgd,slkd->skgl/dot_general | solution.py:80
  17.0 1.4 fusion.51
  18.4 0.1 reshape.432
  18.5 0.2 fusion.122
  18.7 14.5 %all-reduce.5 = bf16[16,2048]{1,0:T(8,128)(2,1)S(1)} all-reduce(f32[16,2048]{1,0:T(8,128)S(1)} %fusion.122), channel_id=1, replica_groups=mesh['ep'=8,'tp'=4] {'tp'}, use_global_device_ids=true, to_apply=%region_2.3 | all-reduce | flops 32768 | bytes 196608 | tf_op jit(solution)/shard_map/psum | solution.py:113
  33.2 0.1 multiply_reduce_fusion.1
  33.3 0.1 copy.48
  33.4 0.1 eq.37
  33.5 0.1 fusion.93
  33.6 0.1 copy.49
  33.7 0.1 reduce_window_sum.11
  33.8 0.2 select_reduce_fusion
  34.0 0.2 multiply_reduce_fusion.2
  34.2 0.1 reshape.433
  34.3 0.1 multiply_convert_fusion
  34.4 1.7 %gather_fusion = bf16[128,2048]{1,0:T(8,128)(2,1)} fusion(bf16[16,2048]{1,0:T(8,128)(2,1)S(1)} %multiply_convert_fusion, s32[1024]{0:T(1024)S(1)} %pad_clamp_fusion.1), kind=kCustom, calls=%fused_computation | custom fusion | bytes 1049088 | tf_op jit(solution)/shard_map/gather | solution.py:134
  36.1 5.8 %all-to-all-start = ((bf16[8,16,2048]{2,1,0:T(8,128)(2,1)}), bf16[8,16,2048]{2,1,0:T(8,128)(2,1)S(1)}, u32[]{:S(2)}, u32[]{:S(2)}) async-start(bf16[8,16,2048]{2,1,0:T(8,128)(2,1)} %bitcast.7), calls=%async_computation | async-start | bytes 1048576 | tf_op jit(solution)/shard_map/all_to_all | solution.py:135
  41.9 0.0 reduce-scatter.2.cloned.1.call-start
  42.0 13.4 %all-to-all-done = bf16[8,16,2048]{2,1,0:T(8,128)(2,1)S(1)} async-done(((bf16[8,16,2048]{2,1,0:T(8,128)(2,1)}), bf16[8,16,2048]{2,1,0:T(8,128)(2,1)S(1)}, u32[]{:S(2)}, u32[]{:S(2)}) %all-to-all-start) | async-done | bytes 524320 | tf_op jit(solution)/shard_map/all_to_all | solution.py:135
  55.4 2.0 %fusion.14 = f32[8,1,16,512]{3,2,0,1:T(8,128)S(1)} fusion(bf16[8,16,2048]{2,1,0:T(8,128)(2,1)S(1)} %all-to-all-done, bf16[1,2048,512]{2,1,0:T(8,128)(2,1)} %param.35), kind=kOutput, calls=%fused_computation.16 | convolution fusion | flops 268500992 | bytes 2883584 | tf_op jit(solution)/shard_map/sjnd,jdf->sjnf/dot_general | solution.py:138
  57.4 3.2 %convolution_convert_fusion = bf16[8,16,2048]{2,1,0:T(8,128)(2,1)} fusion(bf16[1,512,2048]{2,1,0:T(8,128)(2,1)S(1)} %copy-done, bf16[8,16,2048]{2,1,0:T(8,128)(2,1)S(1)} %all-to-all-done, bf16[1,2048,512]{2,1,0:T(8,128)(2,1)} %param.36, f32[8,1,16,512]{3,2,0,1:T(8,128)S(1)} %fusion.14), kind=kOutput, calls=%fused_computation.9 | convolution fusion | flops 537722880 | bytes 5505024 | tf_op jit(solution)/shard_map/sjnf,jfd->sjnd/dot_general | solution.py:143
  60.7 0.0 reduce-scatter.2.cloned.1.call-update
  60.7 0.7 stack.2
  61.4 3.7 %all-to-all-start.3 = ((bf16[8,4,2048]{2,1,0:T(4,128)(2,1)}), bf16[8,4,2048]{2,1,0:T(4,128)(2,1)S(1)}, u32[]{:S(2)}, u32[]{:S(2)}) async-start(bf16[8,4,2048]{2,1,0:T(4,128)(2,1)} %stack.2), calls=%async_computation.4 | async-start | bytes 262144 | tf_op jit(solution)/shard_map/all_to_all | solution.py:119
  65.1 0.1 reshape.440
  65.2 0.1 reshape.441
  65.3 0.1 copy.47
  65.4 7.0 %all-to-all-done.3 = bf16[8,4,2048]{2,1,0:T(4,128)(2,1)S(1)} async-done(((bf16[8,4,2048]{2,1,0:T(4,128)(2,1)}), bf16[8,4,2048]{2,1,0:T(4,128)(2,1)S(1)}, u32[]{:S(2)}, u32[]{:S(2)}) %all-to-all-start.3) | async-done | bytes 131104 | tf_op jit(solution)/shard_map/all_to_all | solution.py:119
  72.5 2.0 %convolution_minimum_fusion = f32[32,512]{1,0:T(8,128)S(1)} fusion(bf16[32,2048]{1,0:T(8,128)(2,1)S(1)} %reshape.442, bf16[2048,512]{1,0:T(8,128)(2,1)} %param.38), kind=kOutput, calls=%fused_computation.29 | convolution fusion | flops 67125248 | bytes 2293760 | tf_op jit(solution)/shard_map/dot_general | solution.py:120
  74.5 7.3 %reduce-scatter.2.cloned.1.call-done = bf16[8,16,512]{2,1,0:T(8,128)(2,1)} async-done(((bf16[8,16,2048]{2,1,0:T(8,128)(2,1)}), bf16[8,16,512]{2,1,0:T(8,128)(2,1)}) %reduce-scatter.2.cloned.1.call-update) | async-done | bytes 131088 | tf_op jit(solution)/shard_map/reduce_scatter | solution.py:148
  81.8 5.5 %all-to-all-start.1 = ((bf16[8,16,512]{2,1,0:T(8,128)(2,1)}), bf16[8,16,512]{2,1,0:T(8,128)(2,1)S(1)}, u32[]{:S(2)}, u32[]{:S(2)}) async-start(bf16[8,16,512]{2,1,0:T(8,128)(2,1)} %reduce-scatter.2.cloned.1.call-done), calls=%async_computation.2 | async-start | bytes 262144 | tf_op jit(solution)/shard_map/all_to_all | solution.py:151
  87.3 0.0 copy-start.15
  87.3 0.0 all-reduce.4.cloned.1.call-start
  87.4 3.8 %fusion.47 = f32[32,2048]{1,0:T(8,128)} fusion(bf16[512,2048]{1,0:T(8,128)(2,1)} %param.40, bf16[32,2048]{1,0:T(8,128)(2,1)S(1)} %reshape.442, bf16[2048,512]{1,0:T(8,128)(2,1)} %param.39, f32[32,512]{1,0:T(8,128)S(1)} %convolution_minimum_fusion), kind=kOutput, calls=%fused_computation.31 | convolution fusion | flops 134365184 | bytes 4653056 | tf_op jit(solution)/shard_map/dot_general | solution.py:124
  91.2 0.0 all-reduce.4.cloned.1.call-update
  91.2 3.4 %all-to-all-done.1 = bf16[8,16,512]{2,1,0:T(8,128)(2,1)S(1)} async-done(((bf16[8,16,512]{2,1,0:T(8,128)(2,1)}), bf16[8,16,512]{2,1,0:T(8,128)(2,1)S(1)}, u32[]{:S(2)}, u32[]{:S(2)}) %all-to-all-start.1) | async-done | bytes 131104 | tf_op jit(solution)/shard_map/all_to_all | solution.py:151
  94.7 0.7 gather_fusion.1
  95.4 0.2 multiply_reduce_fusion
  95.6 0.6 convert_element_type.115
  96.2 3.3 %all-to-all-start.2 = ((bf16[4,4,512]{2,1,0:T(4,128)(2,1)}), bf16[4,4,512]{2,1,0:T(4,128)(2,1)S(1)}, u32[]{:S(2)}, u32[]{:S(2)}) async-start(bf16[4,4,512]{2,1,0:T(4,128)(2,1)} %convert_element_type.115), calls=%async_computation.3 | async-start | bytes 32768 | tf_op jit(solution)/shard_map/all_to_all | solution.py:156
  99.5 0.1 fusion.60
  99.6 0.1 copy-done.15
  99.7 0.7 dynamic-slice
  101.0 2.3 %all-to-all-done.2 = bf16[4,4,512]{2,1,0:T(4,128)(2,1)S(1)} async-done(((bf16[4,4,512]{2,1,0:T(4,128)(2,1)}), bf16[4,4,512]{2,1,0:T(4,128)(2,1)S(1)}, u32[]{:S(2)}, u32[]{:S(2)}) %all-to-all-start.2) | async-done | bytes 16416 | tf_op jit(solution)/shard_map/all_to_all | solution.py:156
  103.3 59.2 %all-reduce.4.cloned.1.call-done = f32[32,2048]{1,0:T(8,128)} async-done(((f32[32,2048]{1,0:T(8,128)}), f32[32,2048]{1,0:T(8,128)}) %all-reduce.4.cloned.1.call-update) | async-done | bytes 262160
  162.5 1.5 fusion.88
  (47 shorter events, 0.3 us)
Async XLA Ops:
  7.4 50.1 %copy-start = (bf16[1,512,2048]{2,1,0:T(8,128)(2,1)S(1)}, bf16[1,512,2048]{2,1,0:T(8,128)(2,1)}, u32[]{:S(2)}) copy-start(bf16[1,512,2048]{2,1,0:T(8,128)(2,1)} %param.37) | copy-start | bytes 6291460
  9.8 2.1 %copy-start.2 = (bf16[16,2048]{1,0:T(8,128)(2,1)S(1)}, bf16[16,2048]{1,0:T(8,128)(2,1)}, u32[]{:S(2)}) copy-start(bf16[16,2048]{1,0:T(8,128)(2,1)} %param.21) | copy-start | bytes 196612
  9.8 2.2 %copy-start.4 = (bf16[2048,128]{1,0:T(8,128)(2,1)S(1)}, bf16[2048,128]{1,0:T(8,128)(2,1)}, u32[]{:S(2)}) copy-start(bf16[2048,128]{1,0:T(8,128)(2,1)} %param.23) | copy-start | bytes 1572868
  9.8 2.2 %copy-start.5 = (f32[2048]{0:T(1024)S(1)}, f32[2048]{0:T(1024)}, u32[]{:S(2)}) copy-start(f32[2048]{0:T(1024)} %param.22) | copy-start | bytes 24580
  9.9 2.5 %copy-start.12 = (bf16[2048,2]{0,1:T(2,128)(2,1)S(1)}, bf16[2048,2]{0,1:T(2,128)(2,1)}, u32[]{:S(2)}) copy-start(bf16[2048,2]{0,1:T(2,128)(2,1)} %param.26) | copy-start | bytes 24580
  9.9 2.5 %copy-start.14 = (f32[2]{0:T(128)S(1)}, f32[2]{0:T(128)}, u32[]{:S(2)}) copy-start(f32[2]{0:T(128)} %param.27) | copy-start | bytes 28
  9.9 2.8 %copy-start.10 = (bf16[2048,64]{0,1:T(8,128)(2,1)S(1)}, bf16[2048,64]{0,1:T(8,128)(2,1)}, u32[]{:S(2)}) copy-start(bf16[2048,64]{0,1:T(8,128)(2,1)} %param.24) | copy-start | bytes 786436
  9.9 3.0 %copy-start.11 = (bf16[2048,64]{0,1:T(8,128)(2,1)S(1)}, bf16[2048,64]{0,1:T(8,128)(2,1)}, u32[]{:S(2)}) copy-start(bf16[2048,64]{0,1:T(8,128)(2,1)} %param.25) | copy-start | bytes 786436
  9.9 3.4 %copy-start.1 = (f32[16,2,1024]{2,1,0:T(2,128)S(1)}, f32[16,2,1024]{2,1,0:T(2,128)}, u32[]{:S(2)}) copy-start(f32[16,2,1024]{2,1,0:T(2,128)} %param.30) | copy-start | bytes 393220
  13.3 3.7 %copy-start.9 = (bf16[16,1024,1,128]{3,1,2,0:T(8,128)(2,1)S(1)}, bf16[16,1024,1,128]{3,1,2,0:T(8,128)(2,1)}, u32[]{:S(2)}) copy-start(bf16[16,1024,1,128]{3,1,2,0:T(8,128)(2,1)} %param.29) | copy-start | bytes 12582916
  17.0 1.5 copy-start.3
  17.0 16.3 %copy-start.7 = (s32[16,4]{0,1:T(4,128)S(1)}, s32[16,4]{0,1:T(4,128)}, u32[]{:S(2)}) copy-start(s32[16,4]{0,1:T(4,128)} %param.33) | copy-start | bytes 772
  17.0 17.3 %copy-start.6 = (f32[2048]{0:T(1024)S(1)}, f32[2048]{0:T(1024)}, u32[]{:S(2)}) copy-start(f32[2048]{0:T(1024)} %param.32) | copy-start | bytes 24580
  36.1 19.3 %all-to-all-start = ((bf16[8,16,2048]{2,1,0:T(8,128)(2,1)}), bf16[8,16,2048]{2,1,0:T(8,128)(2,1)S(1)}, u32[]{:S(2)}, u32[]{:S(2)}) async-start(bf16[8,16,2048]{2,1,0:T(8,128)(2,1)} %bitcast.7), calls=%async_computation | async-start | bytes 1048576 | tf_op jit(solution)/shard_map/all_to_all | solution.py:135
  41.9 39.9 %reduce-scatter.2.cloned.1.call-start = ((), (), s32[]{:S(2)}) async-start(), calls=%async_computation.5 | async-start | bytes 655360 | tf_op jit(solution)/shard_map/reduce_scatter | solution.py:148
  57.4 7.9 %copy-start.8 = (f32[16,4]{0,1:T(4,128)S(1)}, f32[16,4]{0,1:T(4,128)}, u32[]{:S(2)}) copy-start(f32[16,4]{0,1:T(4,128)} %param.34) | copy-start | bytes 772
  61.4 11.0 %all-to-all-start.3 = ((bf16[8,4,2048]{2,1,0:T(4,128)(2,1)}), bf16[8,4,2048]{2,1,0:T(4,128)(2,1)S(1)}, u32[]{:S(2)}, u32[]{:S(2)}) async-start(bf16[8,4,2048]{2,1,0:T(4,128)(2,1)} %stack.2), calls=%async_computation.4 | async-start | bytes 262144 | tf_op jit(solution)/shard_map/all_to_all | solution.py:119
  81.8 12.9 %all-to-all-start.1 = ((bf16[8,16,512]{2,1,0:T(8,128)(2,1)}), bf16[8,16,512]{2,1,0:T(8,128)(2,1)S(1)}, u32[]{:S(2)}, u32[]{:S(2)}) async-start(bf16[8,16,512]{2,1,0:T(8,128)(2,1)} %reduce-scatter.2.cloned.1.call-done), calls=%async_computation.2 | async-start | bytes 262144 | tf_op jit(solution)/shard_map/all_to_all | solution.py:151
  87.3 12.1 %copy-start.13 = (f32[2048]{0:T(1024)S(1)}, f32[2048]{0:T(1024)}, u32[]{:S(2)}) copy-start(f32[2048]{0:T(1024)} %param.41) | copy-start | bytes 24580
  87.3 12.3 %copy-start.15 = (u32[32]{0:T(128)S(1)}, u32[32]{0:T(128)}, u32[]{:S(2)}) copy-start(u32[32]{0:T(128)} %constant.108) | copy-start | bytes 388
  87.3 75.1 %all-reduce.4.cloned.1.call-start = ((), (), s32[]{:S(2)}) async-start(), calls=%async_computation.6 | async-start | bytes 524288
  96.2 7.1 %all-to-all-start.2 = ((bf16[4,4,512]{2,1,0:T(4,128)(2,1)}), bf16[4,4,512]{2,1,0:T(4,128)(2,1)S(1)}, u32[]{:S(2)}, u32[]{:S(2)}) async-start(bf16[4,4,512]{2,1,0:T(4,128)(2,1)} %convert_element_type.115), calls=%async_computation.3 | async-start | bytes 32768 | tf_op jit(solution)/shard_map/all_to_all | solution.py:156
Sparse Core Ops, SparseCore 0:
  60.8 20.9 reduce-scatter.1
Sparse Core Ops, SparseCore 1:
  91.3 71.1 all-reduce.3
